TPU v7x, 128 devices: a whole 4x4x4 slice. The times are simulated.
128 devices in a mesh: sp: 16 (over z, y), dp: 8 (over x, core).
Axes of the slice: x: 4, y: 4, z: 4, core: 2. Of those that a mesh axis runs over, the one named last changes fastest.
Arguments:
- query: bfloat16 [8, 3072, 3072], P('dp', 'sp'), may hold values from -18 to 18
- latent: bfloat16 [8, 3072, 1024], P('dp', 'sp'), may hold values from -6 to 6
- rope_key: bfloat16 [8, 3072, 32], P('dp', 'sp'), may hold values from -5 to 5
- latent_norm_gain: float32 [1024], replicated, may hold values from 0.1 to 1.9
- key_up_matrix: bfloat16 [2048, 1024], P('dp'), may hold values from -0.1875 to 0.1875
- value_up_matrix: bfloat16 [2048, 1024], P('dp'), may hold values from -0.1875 to 0.1875
- out_grad: bfloat16 [8, 3072, 2048], P('dp', 'sp'), may hold values from -6 to 6
Outputs:
- query_grad: bfloat16 [8, 3072, 3072], P('dp', 'sp')
- latent_grad: float32 [8, 3072, 1024], P('dp', 'sp')
- rope_key_grad: float32 [8, 3072, 32], P('dp', 'sp')
- key_weight_grad: float32 [2048, 1024], P('dp')
- value_weight_grad: float32 [2048, 1024], P('dp')
- gain_grad: float32 [1024], replicated
All inputs are finite; a program needn't handle non-finite values.
Results may differ from a plain program's by a relative error of at most 0.011.
Values may be sent and summed in bfloat16 or wider, within the bound.
A program may use at most 256 MiB of HBM per device.

v0:
```python
import functools
import jax
import jax.numpy as jnp
from jax import lax
from jax.sharding import Mesh
from jax.sharding import PartitionSpec as P

ATTENTION_HEADS = 32
PLAIN_HEAD_WIDTH = 64
ROPE = 32
VALUE_HEAD_WIDTH = 64
SPAN = 64
DP = ("dp_0", "dp_1")
SP = ("sp_0", "sp_1")
SP_DP = ("sp_0", "sp_1", "dp_0", "dp_1")
eps = 1e-06
rope_base = 10000.0


def from_everyone(value, axis):
    size = lax.axis_size(axis)
    return lax.all_to_all(
        jnp.broadcast_to(value[None], (size, *value.shape)), axis, 0, 0, tiled=True
    )


def in_order(blocks, dim):
    blocks = jnp.moveaxis(blocks, 0, dim)
    shape = blocks.shape
    return blocks.reshape(*shape[:dim], shape[dim] * shape[dim + 1], *shape[dim + 2 :])


def gather_directly(value, axis, dim):
    blocks = from_everyone(value, axis)
    return in_order(blocks, dim)


def split_up(value, dim, size):
    shape = value.shape
    blocks = value.reshape(*shape[:dim], size, shape[dim] // size, *shape[dim + 1 :])
    return jnp.moveaxis(blocks, dim, 0)


def sent_and_summed(value, axis, dim):
    blocks = split_up(value, dim, lax.axis_size(axis))
    arrived = lax.all_to_all(blocks, axis, split_axis=0, concat_axis=0, tiled=True)
    return arrived.sum(axis=0)


def edges_of(length, count):
    unit = 8 if length >= 8 * count else 1
    return [length // unit * k // count * unit for k in range(1, count)]


def all_blocks(value, axes, turns):
    blocks = value[None]
    for k in turns:
        blocks = lax.all_gather(blocks, axes[k], axis=0, tiled=True)
    carried = [lax.axis_size(axes[k]) for k in reversed(turns)]
    blocks = blocks.reshape(*carried, *value.shape)
    turned = sorted(range(len(turns)), key=lambda place: turns[len(turns) - 1 - place])
    return blocks.transpose(*turned, *range(len(turns), blocks.ndim)).reshape(-1, *value.shape)


def gather_all_axes(value, axes, dim):
    numbers = list(range(len(axes)))[::-1]
    widest = value.shape.index(max(value.shape[:-1] or value.shape))
    edges = [0, *edges_of(value.shape[widest], len(axes)), value.shape[widest]]
    finished = []
    for k, (start, end) in enumerate(zip(edges, edges[1:])):
        if end > start:
            section = lax.slice_in_dim(value, start, end, axis=widest)
            finished.append(all_blocks(section, axes, numbers[k:] + numbers[:k]))
    return in_order(jnp.concatenate(finished, axis=widest + 1), dim)


def by_axis(value, axes):
    return functools.reduce(lax.psum, axes, value)


def rotate(values, cosine, sine):
    half = values.shape[-1] // 2
    first = values[..., :half]
    second = values[..., half:]
    return jnp.concatenate(
        [first * cosine - second * sine, second * cosine + first * sine], axis=-1
    )


def angles(length, width):
    inverse = 1.0 / rope_base ** (jnp.arange(0, width, 2, dtype=jnp.float32) / width)
    turned = jnp.arange(length, dtype=jnp.float32)[:, None] * inverse[None, :]
    return (jnp.cos(turned), jnp.sin(turned))


def attend_backward(arrived, rope_full):
    f32 = jnp.float32
    bf16 = jnp.bfloat16
    length = arrived.shape[0]
    local_heads = arrived.shape[1]
    width = PLAIN_HEAD_WIDTH + ROPE
    scale = width ** (-0.5)
    block = 512
    cosine, sine = angles(length, ROPE)
    neg = jnp.finfo(f32).min
    q_nope = arrived[:, :, :PLAIN_HEAD_WIDTH]
    q_rope = rotate(
        arrived[:, :, PLAIN_HEAD_WIDTH:width].astype(f32), cosine[:, None, :], sine[:, None, :]
    ).astype(bf16)
    key_nope = arrived[:, :, width : width + PLAIN_HEAD_WIDTH]
    values = arrived[:, :, width + PLAIN_HEAD_WIDTH : width + PLAIN_HEAD_WIDTH + VALUE_HEAD_WIDTH]
    d_out = arrived[:, :, width + PLAIN_HEAD_WIDTH + VALUE_HEAD_WIDTH :]
    k_rope = rotate(rope_full.astype(f32), cosine, sine).astype(bf16)
    dk_nope = jnp.zeros((length, local_heads, PLAIN_HEAD_WIDTH), f32)
    dk_rope = jnp.zeros((length, ROPE), f32)
    d_vals = jnp.zeros((length, local_heads, VALUE_HEAD_WIDTH), f32)
    dq_parts = []
    for begin in range(0, length, block):
        end = begin + block
        qn = q_nope[begin:end]
        qr = q_rope[begin:end]
        go = d_out[begin:end]
        scores = jnp.einsum("qhd,khd->hqk", qn, key_nope[:end], preferred_element_type=f32)
        scores = (
            scores + jnp.einsum("qhd,kd->hqk", qr, k_rope[:end], preferred_element_type=f32)
        ) * scale
        q_seg = jnp.arange(begin, end) // SPAN
        k_seg = jnp.arange(end) // SPAN
        allowed = k_seg[None, :] <= q_seg[:, None]
        scores = jnp.where(allowed[None], scores, neg)
        probs = jax.nn.softmax(scores, axis=-1)
        d_probs = jnp.einsum("qhd,khd->hqk", go, values[:end], preferred_element_type=f32)
        d_scores = probs * (d_probs - jnp.sum(probs * d_probs, axis=-1, keepdims=True))
        ds_b = d_scores.astype(bf16)
        p_b = probs.astype(bf16)
        dq_n = jnp.einsum("hqk,khd->qhd", ds_b, key_nope[:end], preferred_element_type=f32) * scale
        dq_r = jnp.einsum("hqk,kd->qhd", ds_b, k_rope[:end], preferred_element_type=f32) * scale
        dq_r = rotate(dq_r, cosine[begin:end, None, :], -sine[begin:end, None, :])
        dq_parts.append(jnp.concatenate([dq_n, dq_r], axis=-1).astype(bf16))
        dk_nope = dk_nope.at[:end].add(
            jnp.einsum("hqk,qhd->khd", ds_b, qn, preferred_element_type=f32) * scale
        )
        dk_rope = dk_rope.at[:end].add(
            jnp.einsum("hqk,qhd->kd", ds_b, qr, preferred_element_type=f32) * scale
        )
        d_vals = d_vals.at[:end].add(
            jnp.einsum("hqk,qhd->khd", p_b, go, preferred_element_type=f32)
        )
    query_part = jnp.concatenate(dq_parts, axis=0)
    grads = jnp.concatenate([query_part, dk_nope.astype(bf16), d_vals.astype(bf16)], axis=-1)
    return (grads, rotate(dk_rope, cosine, -sine))


def local(query, latent, rope_key, latent_norm_gain, key_up_matrix, value_up_matrix, out_grad):
    f32 = jnp.float32
    bf16 = jnp.bfloat16
    tokens = latent.shape[1]
    width = PLAIN_HEAD_WIDTH + ROPE
    head_cols = ATTENTION_HEADS * PLAIN_HEAD_WIDTH
    lat = latent[0].astype(f32)
    inv_rms = lax.rsqrt(jnp.mean(lat * lat, axis=-1, keepdims=True) + eps)
    normed = lat * inv_rms
    nlat = (normed * latent_norm_gain).astype(bf16)
    stacked = jnp.stack([key_up_matrix, value_up_matrix])
    whole = lax.all_gather(stacked, DP, axis=1, tiled=True)
    kv_tok = jnp.einsum("tc,gnc->tgn", nlat, whole, preferred_element_type=f32).astype(bf16)
    heads_query = query[0].reshape(tokens, ATTENTION_HEADS, width)
    key_nope = kv_tok[:, 0].reshape(tokens, ATTENTION_HEADS, PLAIN_HEAD_WIDTH)
    values = kv_tok[:, 1].reshape(tokens, ATTENTION_HEADS, VALUE_HEAD_WIDTH)
    d_out = out_grad[0].reshape(tokens, ATTENTION_HEADS, VALUE_HEAD_WIDTH)
    packed = jnp.concatenate([heads_query, key_nope, values, d_out], axis=2)
    arrived = lax.all_to_all(packed, SP, split_axis=1, concat_axis=0, tiled=True)
    rope_full = gather_directly(rope_key[0], SP, 0)
    grads_heads, rope_full_grad = attend_backward(arrived, rope_full)
    returned = lax.all_to_all(grads_heads, SP, split_axis=0, concat_axis=1, tiled=True)
    rope_grad = sent_and_summed(rope_full_grad, SP, 0)
    query_grad = returned[:, :, :width].reshape(tokens, ATTENTION_HEADS * width)
    key_cols = returned[:, :, width : width + PLAIN_HEAD_WIDTH].reshape(tokens, head_cols)
    value_cols = returned[:, :, width + PLAIN_HEAD_WIDTH :].reshape(tokens, head_cols)
    dkv = jnp.stack([key_cols, value_cols], axis=1)
    d_nlat = jnp.einsum("tgn,gnc->tc", dkv, whole, preferred_element_type=f32)
    latents_all = gather_all_axes(nlat[None], DP, 0)
    columns = lax.all_to_all(dkv[None], DP, split_axis=3, concat_axis=0, tiled=True)
    partial_value = jnp.einsum("stgr,stc->grc", columns, latents_all, preferred_element_type=f32)
    weight_grads = lax.psum(partial_value, SP)
    gain_grad = by_axis(jnp.sum(d_nlat * normed, axis=0), SP_DP)
    scaled = d_nlat * latent_norm_gain
    latent_grad = inv_rms * (scaled - normed * jnp.mean(scaled * normed, axis=-1, keepdims=True))
    return (
        query_grad[None],
        latent_grad[None],
        rope_grad[None],
        weight_grads[0],
        weight_grads[1],
        gain_grad,
    )


def solution(mesh):
    split = Mesh(mesh.devices.reshape(4, 4, 4, 2), ("sp_0", "sp_1", "dp_0", "dp_1"))
    in_specs = (
        P(DP, SP, None),
        P(DP, SP, None),
        P(DP, SP, None),
        P(),
        P(DP, None),
        P(DP, None),
        P(DP, SP, None),
    )
    out_specs = (P(DP, SP, None), P(DP, SP, None), P(DP, SP, None), P(DP, None), P(DP, None), P())
    return jax.shard_map(local, mesh=split, in_specs=in_specs, out_specs=out_specs, check_vma=False)
```

profile of v0, /device:TPU:0, one launch (start us, length us, event | category | flops | bytes accessed | tf_op | source)
XLA Modules:
  0.0 623.8 jit_solution(4799579515403184759)
XLA Ops:
  11.1 14.5 %all-gather.2 = bf16[4,96,1024]{2,1,0:T(8,128)(2,1)} all-gather(bf16[1,96,1024]{2,1,0:T(8,128)(2,1)S(1)} %get-tuple-element.261), channel_id=4, replica_groups=mesh['sp_0'=4,'sp_1'=4,'dp_0'=4,'dp_1'=2] {'dp_0'}, dimensions={0}, use_global_device_ids=true | all-gather | bytes 983040 | tf_op jit(solution)/shard_map/all_gather | solution.py:58
  26.4 8.6 %all-to-all-start.1 = ((bf16[16,192,32]{1,2,0:T(8,128)(2,1)}), bf16[16,192,32]{1,2,0:T(8,128)(2,1)S(1)}, u32[]{:S(2)}, u32[]{:S(2)}) async-start(bf16[16,192,32]{1,2,0:T(8,128)(2,1)} %broadcast_in_dim.80), calls=%async_computation.1 | async-start | bytes 524288 | tf_op jit(solution)/shard_map/all_to_all | solution.py:22
  40.2 3.9 reshape_squeeze.12
  45.3 17.1 %all-gather.8.cloned.1.call-done = bf16[2,2048,1024]{2,1,0:T(8,128)(2,1)} async-done(((bf16[2,256,1024]{2,1,0:T(8,128)(2,1)}), bf16[2,2048,1024]{2,1,0:T(8,128)(2,1)}) %all-gather.8.cloned.1.call-update) | async-done | bytes 8388624 | tf_op jit(solution)/shard_map/all_gather | solution.py:165
  62.4 6.2 convolution_convert_fusion
  78.7 5.6 pad_maximum_fusion
  84.4 4.0 copy.83
  88.3 7.2 %all-to-all-start = ((bf16[192,32,288]{2,0,1:T(8,128)(2,1)}), bf16[192,32,288]{2,0,1:T(8,128)(2,1)}, u32[]{:S(2)}, u32[]{:S(2)}) async-start(bf16[192,32,288]{2,0,1:T(8,128)(2,1)} %copy.83), calls=%async_computation | async-start | bytes 9437184 | tf_op jit(solution)/shard_map/all_to_all | solution.py:172
  105.9 61.1 %all-to-all-done = bf16[192,32,288]{2,0,1:T(8,128)(2,1)} async-done(((bf16[192,32,288]{2,0,1:T(8,128)(2,1)}), bf16[192,32,288]{2,0,1:T(8,128)(2,1)}, u32[]{:S(2)}, u32[]{:S(2)}) %all-to-all-start) | async-done | bytes 3538976 | tf_op jit(solution)/shard_map/all_to_all | solution.py:172
  167.0 8.3 %copy.84 = bf16[16,192,2,288]{1,0,3,2:T(8,128)(2,1)} copy(bf16[16,192,2,288]{3,1,2,0:T(8,128)(2,1)} %bitcast.8) | data formatting | bytes 7077888 | tf_op jit(solution)/shard_map/all_to_all | solution.py:172
  175.3 7.2 %all_to_all.48 = bf16[3072,2,288]{0,2,1:T(8,128)(2,1)S(1)} reshape(bf16[16,192,2,288]{1,0,3,2:T(8,128)(2,1)} %copy.84) | data formatting | bytes 7077888 | tf_op jit(solution)/shard_map/all_to_all | solution.py:172
  220.1 5.3 fusion.11
  225.4 7.3 %fusion.297 = (f32[2,512]{1,0:T(2,128)S(1)}, f32[2,512,2048]{2,1,0:T(8,128)S(1)}) fusion(f32[2,512,2048]{2,1,0:T(8,128)} %fusion.11), kind=kOutput, calls=%fused_computation.433 | output fusion | flops 4196351 | bytes 16781312 | tf_op jit(solution)/shard_map/sub | solution.py:131
  232.7 4.1 multiply_reduce_fusion.2
  236.9 4.6 multiply_convert_fusion.2
  247.1 4.3 fusion.9
  251.4 6.3 %fusion.298 = (f32[2,512]{1,0:T(2,128)S(1)}, f32[2,512,2560]{2,1,0:T(8,128)}) fusion(f32[2,512,2560]{2,1,0:T(8,128)S(1)} %fusion.9), kind=kOutput, calls=%fused_computation.434 | output fusion | flops 5245439 | bytes 20975616 | tf_op jit(solution)/shard_map/sub | solution.py:131
  258.5 6.1 multiply_reduce_fusion.1
  276.7 6.1 fusion.7
  282.7 14.9 %fusion.299 = (f32[2,512]{1,0:T(2,128)S(1)}, f32[2,512,3072]{2,1,0:T(8,128)}) fusion(f32[2,512,3072]{2,1,0:T(8,128)} %fusion.7), kind=kOutput, calls=%fused_computation.435 | output fusion | flops 6294527 | bytes 25169920 | tf_op jit(solution)/shard_map/sub | solution.py:131
  297.6 11.8 %multiply_reduce_fusion = (f32[2,512]{1,0:T(2,128)S(1)}, f32[2,512,3072]{2,1,0:T(8,128)}) fusion(f32[2,512,3072]{2,1,0:T(8,128)} %get-tuple-element.301, f32[2,512]{1,0:T(2,128)S(1)} %get-tuple-element.300, bf16[3072,2,288]{0,2,1:T(8,128)(2,1)} %copy-done.6), kind=kOutput, calls=%fused_computation.10 | convolution fusion | flops 412089344 | bytes 26091520 | tf_op jit(solution)/shard_map/qhd,khd->hqk/dot_general | solution.py:132
  309.5 7.4 %multiply_convert_fusion = bf16[2,512,3072]{2,1,0:T(8,128)(2,1)S(1)} fusion(f32[2,512,3072]{2,1,0:T(8,128)} %get-tuple-element.313, f32[2,512]{1,0:T(2,128)S(1)} %get-tuple-element.312, f32[2,512,3072]{2,1,0:T(8,128)S(1)} %bitcast.325, f32[2,512]{1,0:T(2,128)S(1)} %get-tuple-element.300), kind=kLoop, calls=%fused_computation.9 | loop fusion | flops 12582912 | bytes 31465472 | tf_op jit(solution)/shard_map/convert_element_type | solution.py:134
  316.9 3.8 fusion.111
  325.9 6.4 %fusion.99 = f32[3072,2,64]{0,2,1:T(8,128)} fusion(f32[3072,2,64]{0,2,1:T(8,128)} %scatter-add.59, f32[512,2,64]{0,2,1:T(8,128)} %convolution_bitcast_fusion.5, bf16[3072,2,288]{0,2,1:T(8,128)(2,1)} %copy-done.6, f32[2,512]{1,0:T(2,128)S(1)} %get-tuple-element.292, f32[2,512,1024]{2,1,0:T(8,128)} %copy-done.19), kind=kOutput, calls=%fused_computation.121 | convolution fusion | flops 137496576 | bytes 9310208 | tf_op jit(solution)/shard_map/hqk,qhd->khd/dot_general | solution.py:147
  335.3 8.0 %fusion.77 = f32[3072,2,64]{0,2,1:T(8,128)} fusion(f32[3072,2,64]{0,2,1:T(8,128)} %fusion.99, bf16[3072,2,288]{0,2,1:T(8,128)(2,1)} %copy-done.6, f32[2,512]{1,0:T(2,128)S(1)} %get-tuple-element.294, f32[2,512,1536]{2,1,0:T(8,128)} %copy-done.16), kind=kOutput, calls=%fused_computation.91 | convolution fusion | flops 206244352 | bytes 14290944 | tf_op jit(solution)/shard_map/hqk,qhd->khd/dot_general | solution.py:147
  346.1 9.4 %fusion.65 = f32[3072,2,64]{0,2,1:T(8,128)} fusion(f32[3072,2,64]{0,2,1:T(8,128)} %fusion.77, bf16[3072,2,288]{0,2,1:T(8,128)(2,1)} %copy-done.6, f32[2,512]{1,0:T(2,128)S(1)} %get-tuple-element.296, f32[2,512,2048]{2,1,0:T(8,128)} %fusion.11), kind=kOutput, calls=%fused_computation.84 | convolution fusion | flops 274992128 | bytes 19009536 | tf_op jit(solution)/shard_map/hqk,qhd->khd/dot_general | solution.py:147
  355.5 4.4 fusion.70
  359.9 11.3 %fusion.31 = f32[3072,2,64]{0,2,1:T(8,128)} fusion(f32[3072,2,64]{0,2,1:T(8,128)} %fusion.65, bf16[3072,2,288]{0,2,1:T(8,128)(2,1)} %copy-done.6, f32[2,512]{1,0:T(2,128)S(1)} %get-tuple-element.298, f32[2,512,2560]{2,1,0:T(8,128)} %copy-done.3), kind=kOutput, calls=%fused_computation.52 | convolution fusion | flops 343739904 | bytes 23728128 | tf_op jit(solution)/shard_map/hqk,qhd->khd/dot_general | solution.py:147
  371.2 5.1 fusion.24
  376.3 12.7 %fusion.42 = bf16[3072,2,64]{0,2,1:T(8,128)(2,1)} fusion(f32[3072,2,64]{0,2,1:T(8,128)} %fusion.31, bf16[3072,2,288]{0,2,1:T(8,128)(2,1)} %copy-done.6, f32[2,512]{1,0:T(2,128)S(1)} %copy-done.72, f32[2,512,3072]{2,1,0:T(8,128)} %fusion.7), kind=kOutput, calls=%fused_computation.58 | convolution fusion | flops 412880896 | bytes 27660288 | tf_op jit(solution)/shard_map/hqk,qhd->khd/dot_general | solution.py:147
  389.2 4.7 fusion.45
  396.7 8.6 %copy.95 = bf16[3072,2,224]{2,1,0:T(2,128)(2,1)} copy(bf16[3072,2,224]{0,2,1:T(8,128)(2,1)} %pad_maximum_fusion.1) | data formatting | bytes 5505024 | tf_op jit(solution)/shard_map/concatenate | solution.py:150
  405.3 5.1 all-to-all-start.2
  410.5 4.2 copy.123
  424.4 31.9 %all-to-all-done.2 = bf16[3072,2,224]{2,1,0:T(2,128)(2,1)} async-done(((bf16[3072,2,224]{2,1,0:T(2,128)(2,1)}), bf16[3072,2,224]{2,1,0:T(2,128)(2,1)}, u32[]{:S(2)}, u32[]{:S(2)}) %all-to-all-start.2) | async-done | bytes 2752544 | tf_op jit(solution)/shard_map/all_to_all | solution.py:175
  475.5 6.1 copy.105
  481.6 4.4 all-to-all-start.4
  488.4 3.9 fusion.85
  492.3 4.3 fusion.50
  498.8 14.3 %all-to-all-done.4 = bf16[1,192,2,2048]{1,2,0,3:T(2,128)(2,1)} async-done(((bf16[1,192,2,2048]{1,2,0,3:T(2,128)(2,1)}), bf16[1,192,2,2048]{1,2,0,3:T(2,128)(2,1)}, u32[]{:S(2)}, u32[]{:S(2)}) %all-to-all-start.4) | async-done | bytes 1572896 | tf_op jit(solution)/shard_map/all_to_all | solution.py:183
  513.1 3.9 copy.120
  517.0 4.6 fusion.90
  524.9 19.4 %all_to_all.64 = f32[16,192,32]{1,2,0:T(8,128)} all-to-all(f32[16,192,32]{1,2,0:T(8,128)S(1)} %copy.104), channel_id=1, replica_groups=mesh['sp_0'=4,'sp_1'=4,'dp_0'=4,'dp_1'=2] {'sp_0','sp_1'}, dimensions={0} | all-to-all | bytes 786432 | tf_op jit(solution)/shard_map/all_to_all | solution.py:46
  550.3 5.3 fusion.140
  555.6 8.8 %psum.36 = f32[1024]{0:T(1024)S(1)} all-reduce(f32[1024]{0:T(1024)S(1)} %get-tuple-element.246), channel_id=1, replica_groups=mesh['sp_0'=4,'sp_1'=4,'dp_0'=4,'dp_1'=2] {'sp_0'}, use_global_device_ids=true, to_apply=%region_23.24 | all-reduce | flops 1024 | bytes 8192 | tf_op jit(solution)/shard_map/psum | solution.py:78
  564.4 8.7 %psum.37 = f32[1024]{0:T(1024)S(1)} all-reduce(f32[1024]{0:T(1024)S(1)} %psum.36), channel_id=1, replica_groups=mesh['sp_0'=4,'sp_1'=4,'dp_0'=4,'dp_1'=2] {'sp_1'}, use_global_device_ids=true, to_apply=%region_24.25 | all-reduce | flops 1024 | bytes 8192 | tf_op jit(solution)/shard_map/psum | solution.py:78
  573.2 9.4 %psum.38 = f32[1024]{0:T(1024)S(1)} all-reduce(f32[1024]{0:T(1024)S(1)} %psum.37), channel_id=1, replica_groups=mesh['sp_0'=4,'sp_1'=4,'dp_0'=4,'dp_1'=2] {'dp_0'}, use_global_device_ids=true, to_apply=%region_25.26 | all-reduce | flops 1024 | bytes 8192 | tf_op jit(solution)/shard_map/psum | solution.py:78
  586.8 27.2 %all-reduce.5.cloned.1.call-done = f32[2,256,1024]{2,1,0:T(8,128)} async-done(((f32[2,256,1024]{2,1,0:T(8,128)}), f32[2,256,1024]{2,1,0:T(8,128)}) %all-reduce.5.cloned.1.call-update) | async-done | bytes 2097168 | tf_op jit(solution)/shard_map/psum | solution.py:185
  (298 shorter events, 150.8 us)
Async XLA Ops:
  7.2 18.4 %copy-start.73 = (bf16[1,192,32]{1,2,0:T(8,128)(2,1)S(1)}, bf16[1,192,32]{1,2,0:T(8,128)(2,1)}, u32[]{:S(2)}) copy-start(bf16[1,192,32]{1,2,0:T(8,128)(2,1)} %param.51) | copy-start | bytes 36868
  7.2 55.2 %all-gather.8.cloned.1.call-start = ((), (), s32[]{:S(2)}) async-start(), calls=%async_computation.5 | async-start | bytes 9437184 | tf_op jit(solution)/shard_map/all_gather | solution.py:165
  9.6 28.7 %copy-start.41 = (bf16[1,192,2048]{2,1,0:T(8,128)(2,1)S(1)}, bf16[1,192,2048]{2,1,0:T(8,128)(2,1)}, u32[]{:S(2)}) copy-start(bf16[1,192,2048]{2,1,0:T(8,128)(2,1)} %param.55) | copy-start | bytes 2359300
  9.6 400.9 %all-gather.12.cloned.1.call-start = ((), (), s32[]{:S(2)}) async-start(), calls=%async_computation.8 | async-start | bytes 2359296 | tf_op jit(solution)/shard_map/all_gather | solution.py:58
  10.9 51.5 %copy-start.74 = (f32[192]{0:T(256)}, f32[192]{0:T(256)S(1)}, u32[]{:S(2)}) copy-start(f32[192]{0:T(256)S(1)} %add_rsqrt_fusion) | copy-start | bytes 2308
  26.4 62.0 %all-to-all-start.1 = ((bf16[16,192,32]{1,2,0:T(8,128)(2,1)}), bf16[16,192,32]{1,2,0:T(8,128)(2,1)S(1)}, u32[]{:S(2)}, u32[]{:S(2)}) async-start(bf16[16,192,32]{1,2,0:T(8,128)(2,1)} %broadcast_in_dim.80), calls=%async_computation.1 | async-start | bytes 524288 | tf_op jit(solution)/shard_map/all_to_all | solution.py:22
  35.0 383.5 %all-gather.10.cloned.1.call-start = ((), (), s32[]{:S(2)}) async-start(), calls=%async_computation.7 | async-start | bytes 1966080 | tf_op jit(solution)/shard_map/all_gather | solution.py:58
  88.3 78.7 %all-to-all-start = ((bf16[192,32,288]{2,0,1:T(8,128)(2,1)}), bf16[192,32,288]{2,0,1:T(8,128)(2,1)}, u32[]{:S(2)}, u32[]{:S(2)}) async-start(bf16[192,32,288]{2,0,1:T(8,128)(2,1)} %copy.83), calls=%async_computation | async-start | bytes 9437184 | tf_op jit(solution)/shard_map/all_to_all | solution.py:172
  95.6 8.9 %copy-start.76 = (f32[16]{0:T(128)}, f32[16]{0:T(128)S(1)}, u32[]{:S(2)}) copy-start(f32[16]{0:T(128)S(1)} %negate_power_fusion) | copy-start | bytes 196
  182.5 30.2 %copy-start.6 = (bf16[3072,2,288]{0,2,1:T(8,128)(2,1)}, bf16[3072,2,288]{0,2,1:T(8,128)(2,1)S(1)}, u32[]{:S(2)}) copy-start(bf16[3072,2,288]{0,2,1:T(8,128)(2,1)S(1)} %all_to_all.48) | copy-start | bytes 10616836
  251.4 7.1 %copy-start.3 = (f32[2,512,2560]{2,1,0:T(8,128)}, f32[2,512,2560]{2,1,0:T(8,128)S(1)}, u32[]{:S(2)}) copy-start(f32[2,512,2560]{2,1,0:T(8,128)S(1)} %fusion.9) | copy-start | bytes 31457284
  258.5 6.1 slice-start.5
  258.5 6.7 %slice-start.6 = ((s8[10485760]{0:T(1024)(128)(4,1)}), s8[4194304]{0:T(1024)(128)(4,1)S(1)}, s32[]{:S(2)}) async-start(s8[10485760]{0:T(1024)(128)(4,1)} %bitcast.326), calls=%async_computation.15 | async-start | bytes 8388608
  258.5 7.3 %slice-start.7 = ((s8[10485760]{0:T(1024)(128)(4,1)}), s8[2097152]{0:T(1024)(128)(4,1)S(1)}, s32[]{:S(2)}) async-start(s8[10485760]{0:T(1024)(128)(4,1)} %bitcast.326), calls=%async_computation.16 | async-start | bytes 4194304
  267.7 5.8 copy-start.1
  297.6 11.8 %copy-start.71 = (f32[2,512]{1,0:T(2,128)}, f32[2,512]{1,0:T(2,128)S(1)}, u32[]{:S(2)}) copy-start(f32[2,512]{1,0:T(2,128)S(1)} %get-tuple-element.300) | copy-start | bytes 12292
  297.6 11.8 %slice-start.2 = ((s8[12582912]{0:T(1024)(128)(4,1)}), s8[4194304]{0:T(1024)(128)(4,1)S(1)}, s32[]{:S(2)}) async-start(s8[12582912]{0:T(1024)(128)(4,1)} %bitcast.324), calls=%async_computation.11 | async-start | bytes 8388608
  297.6 11.8 %slice-start.3 = ((s8[12582912]{0:T(1024)(128)(4,1)}), s8[4194304]{0:T(1024)(128)(4,1)S(1)}, s32[]{:S(2)}) async-start(s8[12582912]{0:T(1024)(128)(4,1)} %bitcast.324), calls=%async_computation.12 | async-start | bytes 8388608
  297.6 11.8 %slice-start.4 = ((s8[12582912]{0:T(1024)(128)(4,1)}), s8[4194304]{0:T(1024)(128)(4,1)S(1)}, s32[]{:S(2)}) async-start(s8[12582912]{0:T(1024)(128)(4,1)} %bitcast.324), calls=%async_computation.13 | async-start | bytes 8388608
  371.2 5.1 copy-start.72
  389.0 5.0 copy-start.50
  389.0 5.0 copy-start.65
  389.0 5.0 copy-start.66
  389.0 5.0 copy-start.55
  389.0 5.0 copy-start.63
  389.0 5.0 copy-start.64
  389.0 5.1 copy-start.51
  389.0 5.1 copy-start.61
  389.1 5.1 copy-start.62
  389.1 5.1 copy-start.52
  389.1 5.1 copy-start.59
  389.1 5.1 copy-start.60
  389.1 5.1 copy-start.53
  389.1 5.1 copy-start.57
  389.1 5.1 copy-start.58
  389.1 5.1 copy-start.45
  389.1 5.2 copy-start.46
  389.1 5.2 copy-start.48
  389.2 5.2 copy-start.49
  405.3 50.9 %all-to-all-start.2 = ((bf16[3072,2,224]{2,1,0:T(2,128)(2,1)}), bf16[3072,2,224]{2,1,0:T(2,128)(2,1)}, u32[]{:S(2)}, u32[]{:S(2)}) async-start(bf16[3072,2,224]{2,1,0:T(2,128)(2,1)} %copy.95), calls=%async_computation.2 | async-start | bytes 6291456 | tf_op jit(solution)/shard_map/all_to_all | solution.py:175
  414.7 7.3 %copy-start.10 = (bf16[3072,2,16]{0,2,1:T(8,128)(2,1)S(1)}, bf16[3072,2,16]{0,2,1:T(8,128)(2,1)}, u32[]{:S(2)}) copy-start(bf16[3072,2,16]{0,2,1:T(8,128)(2,1)} %copy-done.8) | copy-start | bytes 589828
  414.7 7.3 %copy-start.13 = (bf16[3072,2,16]{0,2,1:T(8,128)(2,1)S(1)}, bf16[3072,2,16]{0,2,1:T(8,128)(2,1)}, u32[]{:S(2)}) copy-start(bf16[3072,2,16]{0,2,1:T(8,128)(2,1)} %copy-done.11) | copy-start | bytes 589828
  481.6 31.5 %all-to-all-start.4 = ((bf16[1,192,2,2048]{1,2,0,3:T(2,128)(2,1)}), bf16[1,192,2,2048]{1,2,0,3:T(2,128)(2,1)}, u32[]{:S(2)}, u32[]{:S(2)}) async-start(bf16[1,192,2,2048]{1,2,0,3:T(2,128)(2,1)} %copy.105), calls=%async_computation.4 | async-start | bytes 4194304 | tf_op jit(solution)/shard_map/all_to_all | solution.py:183
  485.9 128.1 %all-reduce.5.cloned.1.call-start = ((), (), s32[]{:S(2)}) async-start(), calls=%async_computation.6 | async-start | bytes 4194304 | tf_op jit(solution)/shard_map/psum | solution.py:185
  486.0 10.6 %slice-start = ((s8[6291456]{0:T(1024)(128)(4,1)}), s8[4194304]{0:T(1024)(128)(4,1)S(1)}, s32[]{:S(2)}) async-start(s8[6291456]{0:T(1024)(128)(4,1)} %bitcast.322), calls=%async_computation.9 | async-start | bytes 8388608
  488.4 8.2 %slice-start.1 = ((s8[6291456]{0:T(1024)(128)(4,1)}), s8[2097152]{0:T(1024)(128)(4,1)S(1)}, s32[]{:S(2)}) async-start(s8[6291456]{0:T(1024)(128)(4,1)} %bitcast.322), calls=%async_computation.10 | async-start | bytes 4194304
  498.8 18.2 %copy-start.39 = (bf16[8,1,96,1024]{3,0,2,1:T(8,128)(2,1)S(1)}, bf16[8,1,96,1024]{3,0,2,1:T(8,128)(2,1)}, u32[]{:S(2)}) copy-start(bf16[8,1,96,1024]{3,0,2,1:T(8,128)(2,1)} %reshape.969) | copy-start | bytes 4718596
  521.6 24.4 %copy-start.18 = (bf16[192,16,2,224]{3,0,2,1:T(8,128)(2,1)S(1)}, bf16[192,16,2,224]{3,0,2,1:T(8,128)(2,1)}, u32[]{:S(2)}) copy-start(bf16[192,16,2,224]{3,0,2,1:T(8,128)(2,1)} %copy-done.17) | copy-start | bytes 8257540
  (46 other events, 132.4 us)
Sparse Core Ops, SparseCore 0:
  10.3 52.0 all-gather.7
  64.1 12.6 all-gather.11
  78.4 27.7 all-gather.9
  521.7 92.2 all-reduce.4
where the time goes:
time: 634 us; the launch traced here: 624 us
  matrix products  182 us (29%)
  waiting for transfers between devices  152 us (24%)
  local copies, waits for them, and re-layouts  105 us (17%)
  other arithmetic  78.7 us (12%)
  blocking collectives  66.1 us (10%)
  starting transfers between devices  25.5 us (4%)
  between operations  15.3 us (2%)
    all_to_all x1, waiting for transfers between devices, local(): lax.all_to_all(packed, SP, split_axis=1, concat_axis=0, tiled=True)  61.1 us
    dot_general x6, matrix products, attend_backward(): jnp.einsum('hqk,qhd->khd', p_b, go, preferred_element_type=f32)  51.5 us
    sub x6, other arithmetic, attend_backward(): probs = jax.nn.softmax(scores, axis=-1)  32.6 us
    all_to_all x1, waiting for transfers between devices, local(): lax.all_to_all(grads_heads, SP, split_axis=0, concat_axis=1, tiled=True)  31.9 us
    psum x4, blocking collectives, by_axis(): return functools.reduce(lax.psum, axes, value)  30 us
    psum x1, waiting for transfers between devices, local(): weight_grads = lax.psum(partial_value, SP)  27.2 us
    dot_general x6, matrix products, attend_backward(): jnp.einsum('qhd,khd->hqk', go, values[:end], preferred_element_type=f32)  27.1 us
    dot_general x6, matrix products, attend_backward(): jnp.einsum('hqk,qhd->khd', ds_b, qn, preferred_element_type=f32) * scale  21.1 us
  transfers between devices with their start and end apart: 8, of which 5 were waited for; matrix products, arithmetic and copies ran while one was open for 50% of the time, Pallas kernels for 0%

commit v1 on v0

--- a/solution.py
+++ b/solution.py
@@ -172,7 +172,9 @@
     arrived = lax.all_to_all(packed, SP, split_axis=1, concat_axis=0, tiled=True)
     rope_full = gather_directly(rope_key[0], SP, 0)
     grads_heads, rope_full_grad = attend_backward(arrived, rope_full)
-    returned = lax.all_to_all(grads_heads, SP, split_axis=0, concat_axis=1, tiled=True)
+    cells = jnp.split(grads_heads, lax.axis_size(SP), axis=0)
+    received = lax.all_to_all(jnp.stack(cells), SP, 0, 0)
+    returned = jnp.concatenate(received, axis=1)
     rope_grad = sent_and_summed(rope_full_grad, SP, 0)
     query_grad = returned[:, :, :width].reshape(tokens, ATTENTION_HEADS * width)
     key_cols = returned[:, :, width : width + PLAIN_HEAD_WIDTH].reshape(tokens, head_cols)

time: 634 us -> 640 us (level)
  local copies, waits for them, and re-layouts: 105 us -> 112 us
    unnamed x173 -> x184, local copies, waits for them, and re-layouts: 10.8 us -> 26 us
    concatenate x1 -> x0, local copies, waits for them, and re-layouts: 8.61 us -> none  [attend_backward(): jnp.concatenate([query_part, dk_nope.astype(bf16), d_vals.astype(bf16)],...]
    another operation x0 -> x2, local copies, waits for them, and re-layouts: none -> 6.79 us  [local(): received = lax.all_to_all(jnp.stack(cells), SP, 0, 0)]
  transfers between devices with their start and end apart: 8 -> 8, of which waited for: 5 -> 5; matrix products, arithmetic and copies ran while one was open for 50% -> 51% of each run, Pallas kernels for 0% -> 0%
where the time goes in v1:
time: 640 us; the launch traced here: 630 us
  matrix products  183 us (29%)
  waiting for transfers between devices  150 us (23%)
  local copies, waits for them, and re-layouts  112 us (18%)
  other arithmetic  76.6 us (12%)
  blocking collectives  66.1 us (10%)
  starting transfers between devices  25.9 us (4%)
  between operations  15.3 us (2%)
    all_to_all x1, waiting for transfers between devices, local(): lax.all_to_all(packed, SP, split_axis=1, concat_axis=0, tiled=True)  61.1 us
    dot_general x6, matrix products, attend_backward(): jnp.einsum('hqk,qhd->khd', p_b, go, preferred_element_type=f32)  51.8 us
    sub x6, other arithmetic, attend_backward(): probs = jax.nn.softmax(scores, axis=-1)  32.7 us
    all_to_all x1, waiting for transfers between devices, local(): received = lax.all_to_all(jnp.stack(cells), SP, 0, 0)  30.7 us
    psum x4, blocking collectives, by_axis(): return functools.reduce(lax.psum, axes, value)  28.8 us
    psum x1, waiting for transfers between devices, local(): weight_grads = lax.psum(partial_value, SP)  28.2 us
    dot_general x6, matrix products, attend_backward(): jnp.einsum('qhd,khd->hqk', go, values[:end], preferred_element_type=f32)  27.2 us
    unnamed x184, local copies, waits for them, and re-layouts  26 us
  transfers between devices with their start and end apart: 8, of which 5 were waited for; matrix products, arithmetic and copies ran while one was open for 51% of the time, Pallas kernels for 0%

profile of v1, /device:TPU:0, one launch (start us, length us, event | category | flops | bytes accessed | tf_op | source)
XLA Modules:
  0.0 629.6 jit_solution(11218883314387294186)
XLA Ops:
  11.7 15.0 %all-gather.2 = bf16[4,96,1024]{2,1,0:T(8,128)(2,1)} all-gather(bf16[1,96,1024]{2,1,0:T(8,128)(2,1)S(1)} %get-tuple-element.261), channel_id=4, replica_groups=mesh['sp_0'=4,'sp_1'=4,'dp_0'=4,'dp_1'=2] {'dp_0'}, dimensions={0}, use_global_device_ids=true | all-gather | bytes 983040 | tf_op jit(solution)/shard_map/all_gather | solution.py:58
  27.5 8.5 %all-to-all-start.1 = ((bf16[16,192,32]{1,2,0:T(8,128)(2,1)}), bf16[16,192,32]{1,2,0:T(8,128)(2,1)S(1)}, u32[]{:S(2)}, u32[]{:S(2)}) async-start(bf16[16,192,32]{1,2,0:T(8,128)(2,1)} %broadcast_in_dim.80), calls=%async_computation.1 | async-start | bytes 524288 | tf_op jit(solution)/shard_map/all_to_all | solution.py:22
  41.3 3.9 reshape_squeeze.12
  46.3 16.1 %all-gather.8.cloned.1.call-done = bf16[2,2048,1024]{2,1,0:T(8,128)(2,1)} async-done(((bf16[2,256,1024]{2,1,0:T(8,128)(2,1)}), bf16[2,2048,1024]{2,1,0:T(8,128)(2,1)}) %all-gather.8.cloned.1.call-update) | async-done | bytes 8388624 | tf_op jit(solution)/shard_map/all_gather | solution.py:165
  62.4 6.2 convolution_convert_fusion
  78.7 5.6 pad_maximum_fusion
  84.4 4.0 copy.79
  88.3 7.5 %all-to-all-start = ((bf16[192,32,288]{2,0,1:T(8,128)(2,1)}), bf16[192,32,288]{2,0,1:T(8,128)(2,1)}, u32[]{:S(2)}, u32[]{:S(2)}) async-start(bf16[192,32,288]{2,0,1:T(8,128)(2,1)} %copy.79), calls=%async_computation | async-start | bytes 9437184 | tf_op jit(solution)/shard_map/all_to_all | solution.py:172
  106.3 61.1 %all-to-all-done = bf16[192,32,288]{2,0,1:T(8,128)(2,1)} async-done(((bf16[192,32,288]{2,0,1:T(8,128)(2,1)}), bf16[192,32,288]{2,0,1:T(8,128)(2,1)}, u32[]{:S(2)}, u32[]{:S(2)}) %all-to-all-start) | async-done | bytes 3538976 | tf_op jit(solution)/shard_map/all_to_all | solution.py:172
  167.3 8.3 %copy.80 = bf16[16,192,2,288]{1,0,3,2:T(8,128)(2,1)} copy(bf16[16,192,2,288]{3,1,2,0:T(8,128)(2,1)} %bitcast.8) | data formatting | bytes 7077888 | tf_op jit(solution)/shard_map/all_to_all | solution.py:172
  175.7 7.2 %all_to_all.38 = bf16[3072,2,288]{0,2,1:T(8,128)(2,1)S(1)} reshape(bf16[16,192,2,288]{1,0,3,2:T(8,128)(2,1)} %copy.80) | data formatting | bytes 7077888 | tf_op jit(solution)/shard_map/all_to_all | solution.py:172
  220.4 5.3 fusion.11
  225.7 7.3 %fusion.313 = (f32[2,512]{1,0:T(2,128)S(1)}, f32[2,512,2048]{2,1,0:T(8,128)S(1)}) fusion(f32[2,512,2048]{2,1,0:T(8,128)} %fusion.11), kind=kOutput, calls=%fused_computation.465 | output fusion | flops 4196351 | bytes 16781312 | tf_op jit(solution)/shard_map/sub | solution.py:131
  233.0 4.1 multiply_reduce_fusion.2
  237.2 4.6 multiply_convert_fusion.2
  247.4 4.3 fusion.9
  251.7 6.3 %fusion.314 = (f32[2,512]{1,0:T(2,128)S(1)}, f32[2,512,2560]{2,1,0:T(8,128)}) fusion(f32[2,512,2560]{2,1,0:T(8,128)S(1)} %fusion.9), kind=kOutput, calls=%fused_computation.466 | output fusion | flops 5245439 | bytes 20975616 | tf_op jit(solution)/shard_map/sub | solution.py:131
  258.8 6.1 multiply_reduce_fusion.1
  277.0 6.0 fusion.7
  283.0 14.9 %fusion.315 = (f32[2,512]{1,0:T(2,128)S(1)}, f32[2,512,3072]{2,1,0:T(8,128)}) fusion(f32[2,512,3072]{2,1,0:T(8,128)} %fusion.7), kind=kOutput, calls=%fused_computation.467 | output fusion | flops 6294527 | bytes 25169920 | tf_op jit(solution)/shard_map/sub | solution.py:131
  297.9 11.8 %multiply_reduce_fusion = (f32[2,512]{1,0:T(2,128)S(1)}, f32[2,512,3072]{2,1,0:T(8,128)}) fusion(f32[2,512,3072]{2,1,0:T(8,128)} %get-tuple-element.301, f32[2,512]{1,0:T(2,128)S(1)} %get-tuple-element.300, bf16[3072,2,288]{0,2,1:T(8,128)(2,1)} %copy-done.6), kind=kOutput, calls=%fused_computation.10 | convolution fusion | flops 412089344 | bytes 26091520 | tf_op jit(solution)/shard_map/qhd,khd->hqk/dot_general | solution.py:132
  309.7 7.2 %multiply_convert_fusion = bf16[2,512,3072]{2,1,0:T(8,128)(2,1)S(1)} fusion(f32[2,512,3072]{2,1,0:T(8,128)} %get-tuple-element.313, f32[2,512]{1,0:T(2,128)S(1)} %get-tuple-element.312, f32[2,512,3072]{2,1,0:T(8,128)S(1)} %bitcast.388, f32[2,512]{1,0:T(2,128)S(1)} %get-tuple-element.300), kind=kLoop, calls=%fused_computation.9 | loop fusion | flops 12582912 | bytes 31465472 | tf_op jit(solution)/shard_map/convert_element_type | solution.py:134
  317.0 3.8 fusion.111
  326.1 6.4 %fusion.99 = f32[3072,2,64]{0,2,1:T(8,128)} fusion(f32[3072,2,64]{0,2,1:T(8,128)} %scatter-add.59, f32[512,2,64]{0,2,1:T(8,128)} %convolution_bitcast_fusion.5, bf16[3072,2,288]{0,2,1:T(8,128)(2,1)} %copy-done.6, f32[2,512]{1,0:T(2,128)S(1)} %get-tuple-element.292, f32[2,512,1024]{2,1,0:T(8,128)} %copy-done.16), kind=kOutput, calls=%fused_computation.121 | convolution fusion | flops 137496576 | bytes 9310208 | tf_op jit(solution)/shard_map/hqk,qhd->khd/dot_general | solution.py:147
  335.4 7.9 %fusion.77 = f32[3072,2,64]{0,2,1:T(8,128)} fusion(f32[3072,2,64]{0,2,1:T(8,128)} %fusion.99, bf16[3072,2,288]{0,2,1:T(8,128)(2,1)} %copy-done.6, f32[2,512]{1,0:T(2,128)S(1)} %get-tuple-element.294, f32[2,512,1536]{2,1,0:T(8,128)} %copy-done.15), kind=kOutput, calls=%fused_computation.91 | convolution fusion | flops 206244352 | bytes 14290944 | tf_op jit(solution)/shard_map/hqk,qhd->khd/dot_general | solution.py:147
  346.2 9.5 %fusion.65 = f32[3072,2,64]{0,2,1:T(8,128)} fusion(f32[3072,2,64]{0,2,1:T(8,128)} %fusion.77, bf16[3072,2,288]{0,2,1:T(8,128)(2,1)} %copy-done.6, f32[2,512]{1,0:T(2,128)S(1)} %get-tuple-element.296, f32[2,512,2048]{2,1,0:T(8,128)} %fusion.11), kind=kOutput, calls=%fused_computation.84 | convolution fusion | flops 274992128 | bytes 19009536 | tf_op jit(solution)/shard_map/hqk,qhd->khd/dot_general | solution.py:147
  355.7 4.4 fusion.70
  360.1 11.6 %fusion.31 = f32[3072,2,64]{0,2,1:T(8,128)} fusion(f32[3072,2,64]{0,2,1:T(8,128)} %fusion.65, bf16[3072,2,288]{0,2,1:T(8,128)(2,1)} %copy-done.6, f32[2,512]{1,0:T(2,128)S(1)} %get-tuple-element.298, f32[2,512,2560]{2,1,0:T(8,128)} %copy-done.3), kind=kOutput, calls=%fused_computation.52 | convolution fusion | flops 343739904 | bytes 23728128 | tf_op jit(solution)/shard_map/hqk,qhd->khd/dot_general | solution.py:147
  371.7 5.1 fusion.24
  376.8 12.7 %fusion.42 = bf16[3072,2,64]{0,2,1:T(8,128)(2,1)} fusion(f32[3072,2,64]{0,2,1:T(8,128)} %fusion.31, bf16[3072,2,288]{0,2,1:T(8,128)(2,1)} %copy-done.6, f32[2,512]{1,0:T(2,128)S(1)} %copy-done.69, f32[2,512,3072]{2,1,0:T(8,128)} %fusion.7), kind=kOutput, calls=%fused_computation.58 | convolution fusion | flops 412880896 | bytes 27660288 | tf_op jit(solution)/shard_map/hqk,qhd->khd/dot_general | solution.py:147
  389.8 4.7 fusion.45
  408.2 6.0 copy.91
  414.2 5.3 all-to-all-start.2
  419.6 4.2 copy.119
  434.6 30.7 %all-to-all-done.2 = bf16[16,192,2,224]{3,1,2,0:T(8,128)(2,1)} async-done(((bf16[16,192,2,224]{3,1,2,0:T(8,128)(2,1)}), bf16[16,192,2,224]{3,1,2,0:T(8,128)(2,1)}, u32[]{:S(2)}, u32[]{:S(2)}) %all-to-all-start.2) | async-done | bytes 2752544 | tf_op jit(solution)/shard_map/all_to_all | solution.py:176
  465.3 5.1 fusion.306
  482.6 6.1 copy.99
  488.7 4.4 all-to-all-start.4
  495.5 3.9 fusion.85
  499.4 4.3 fusion.50
  506.1 14.2 %all-to-all-done.4 = bf16[1,192,2,2048]{1,2,0,3:T(2,128)(2,1)} async-done(((bf16[1,192,2,2048]{1,2,0,3:T(2,128)(2,1)}), bf16[1,192,2,2048]{1,2,0,3:T(2,128)(2,1)}, u32[]{:S(2)}, u32[]{:S(2)}) %all-to-all-start.4) | async-done | bytes 1572896 | tf_op jit(solution)/shard_map/all_to_all | solution.py:185
  523.9 4.6 fusion.90
  529.9 20.0 %all_to_all.51 = f32[16,192,32]{1,2,0:T(8,128)S(1)} all-to-all(f32[16,192,32]{1,2,0:T(8,128)S(1)} %copy.98), channel_id=1, replica_groups=mesh['sp_0'=4,'sp_1'=4,'dp_0'=4,'dp_1'=2] {'sp_0','sp_1'}, dimensions={0} | all-to-all | bytes 786432 | tf_op jit(solution)/shard_map/all_to_all | solution.py:46
  556.2 5.3 fusion.140
  561.6 8.3 %psum.36 = f32[1024]{0:T(1024)S(1)} all-reduce(f32[1024]{0:T(1024)S(1)} %get-tuple-element.246), channel_id=1, replica_groups=mesh['sp_0'=4,'sp_1'=4,'dp_0'=4,'dp_1'=2] {'sp_0'}, use_global_device_ids=true, to_apply=%region_23.24 | all-reduce | flops 1024 | bytes 8192 | tf_op jit(solution)/shard_map/psum | solution.py:78
  569.9 9.1 %psum.37 = f32[1024]{0:T(1024)S(1)} all-reduce(f32[1024]{0:T(1024)S(1)} %psum.36), channel_id=1, replica_groups=mesh['sp_0'=4,'sp_1'=4,'dp_0'=4,'dp_1'=2] {'sp_1'}, use_global_device_ids=true, to_apply=%region_24.25 | all-reduce | flops 1024 | bytes 8192 | tf_op jit(solution)/shard_map/psum | solution.py:78
  578.9 8.4 %psum.38 = f32[1024]{0:T(1024)S(1)} all-reduce(f32[1024]{0:T(1024)S(1)} %psum.37), channel_id=1, replica_groups=mesh['sp_0'=4,'sp_1'=4,'dp_0'=4,'dp_1'=2] {'dp_0'}, use_global_device_ids=true, to_apply=%region_25.26 | all-reduce | flops 1024 | bytes 8192 | tf_op jit(solution)/shard_map/psum | solution.py:78
  591.5 28.2 %all-reduce.5.cloned.1.call-done = f32[2,256,1024]{2,1,0:T(8,128)} async-done(((f32[2,256,1024]{2,1,0:T(8,128)}), f32[2,256,1024]{2,1,0:T(8,128)}) %all-reduce.5.cloned.1.call-update) | async-done | bytes 2097168 | tf_op jit(solution)/shard_map/psum | solution.py:187
  (306 shorter events, 158.9 us)
Async XLA Ops:
  7.2 19.6 %copy-start.70 = (bf16[1,192,32]{1,2,0:T(8,128)(2,1)S(1)}, bf16[1,192,32]{1,2,0:T(8,128)(2,1)}, u32[]{:S(2)}) copy-start(bf16[1,192,32]{1,2,0:T(8,128)(2,1)} %param.51) | copy-start | bytes 36868
  7.2 55.2 %all-gather.8.cloned.1.call-start = ((), (), s32[]{:S(2)}) async-start(), calls=%async_computation.5 | async-start | bytes 9437184 | tf_op jit(solution)/shard_map/all_gather | solution.py:165
  9.5 29.8 %copy-start.38 = (bf16[1,192,2048]{2,1,0:T(8,128)(2,1)S(1)}, bf16[1,192,2048]{2,1,0:T(8,128)(2,1)}, u32[]{:S(2)}) copy-start(bf16[1,192,2048]{2,1,0:T(8,128)(2,1)} %param.55) | copy-start | bytes 2359300
  9.6 410.0 %all-gather.12.cloned.1.call-start = ((), (), s32[]{:S(2)}) async-start(), calls=%async_computation.8 | async-start | bytes 2359296 | tf_op jit(solution)/shard_map/all_gather | solution.py:58
  10.8 51.6 %copy-start.71 = (f32[192]{0:T(256)}, f32[192]{0:T(256)S(1)}, u32[]{:S(2)}) copy-start(f32[192]{0:T(256)S(1)} %add_rsqrt_fusion) | copy-start | bytes 2308
  27.5 60.8 %all-to-all-start.1 = ((bf16[16,192,32]{1,2,0:T(8,128)(2,1)}), bf16[16,192,32]{1,2,0:T(8,128)(2,1)S(1)}, u32[]{:S(2)}, u32[]{:S(2)}) async-start(bf16[16,192,32]{1,2,0:T(8,128)(2,1)} %broadcast_in_dim.80), calls=%async_computation.1 | async-start | bytes 524288 | tf_op jit(solution)/shard_map/all_to_all | solution.py:22
  36.0 391.5 %all-gather.10.cloned.1.call-start = ((), (), s32[]{:S(2)}) async-start(), calls=%async_computation.7 | async-start | bytes 1966080 | tf_op jit(solution)/shard_map/all_gather | solution.py:58
  39.3 23.1 %copy-start.66 = (f32[1024]{0:T(1024)S(1)}, f32[1024]{0:T(1024)}, u32[]{:S(2)}) copy-start(f32[1024]{0:T(1024)} %param.52) | copy-start | bytes 12292
  88.3 79.0 %all-to-all-start = ((bf16[192,32,288]{2,0,1:T(8,128)(2,1)}), bf16[192,32,288]{2,0,1:T(8,128)(2,1)}, u32[]{:S(2)}, u32[]{:S(2)}) async-start(bf16[192,32,288]{2,0,1:T(8,128)(2,1)} %copy.79), calls=%async_computation | async-start | bytes 9437184 | tf_op jit(solution)/shard_map/all_to_all | solution.py:172
  95.9 8.9 %copy-start.73 = (f32[16]{0:T(128)}, f32[16]{0:T(128)S(1)}, u32[]{:S(2)}) copy-start(f32[16]{0:T(128)S(1)} %negate_power_fusion) | copy-start | bytes 196
  182.8 30.2 %copy-start.6 = (bf16[3072,2,288]{0,2,1:T(8,128)(2,1)}, bf16[3072,2,288]{0,2,1:T(8,128)(2,1)S(1)}, u32[]{:S(2)}) copy-start(bf16[3072,2,288]{0,2,1:T(8,128)(2,1)S(1)} %all_to_all.38) | copy-start | bytes 10616836
  251.7 7.1 %copy-start.3 = (f32[2,512,2560]{2,1,0:T(8,128)}, f32[2,512,2560]{2,1,0:T(8,128)S(1)}, u32[]{:S(2)}) copy-start(f32[2,512,2560]{2,1,0:T(8,128)S(1)} %fusion.9) | copy-start | bytes 31457284
  258.8 6.1 slice-start.5
  258.8 6.7 %slice-start.6 = ((s8[10485760]{0:T(1024)(128)(4,1)}), s8[4194304]{0:T(1024)(128)(4,1)S(1)}, s32[]{:S(2)}) async-start(s8[10485760]{0:T(1024)(128)(4,1)} %bitcast.389), calls=%async_computation.15 | async-start | bytes 8388608
  258.8 7.3 %slice-start.7 = ((s8[10485760]{0:T(1024)(128)(4,1)}), s8[2097152]{0:T(1024)(128)(4,1)S(1)}, s32[]{:S(2)}) async-start(s8[10485760]{0:T(1024)(128)(4,1)} %bitcast.389), calls=%async_computation.16 | async-start | bytes 4194304
  268.0 5.8 copy-start.1
  297.9 11.8 %copy-start.68 = (f32[2,512]{1,0:T(2,128)}, f32[2,512]{1,0:T(2,128)S(1)}, u32[]{:S(2)}) copy-start(f32[2,512]{1,0:T(2,128)S(1)} %get-tuple-element.300) | copy-start | bytes 12292
  297.9 11.8 %slice-start.2 = ((s8[12582912]{0:T(1024)(128)(4,1)}), s8[4194304]{0:T(1024)(128)(4,1)S(1)}, s32[]{:S(2)}) async-start(s8[12582912]{0:T(1024)(128)(4,1)} %bitcast.387), calls=%async_computation.11 | async-start | bytes 8388608
  297.9 11.8 %slice-start.3 = ((s8[12582912]{0:T(1024)(128)(4,1)}), s8[4194304]{0:T(1024)(128)(4,1)S(1)}, s32[]{:S(2)}) async-start(s8[12582912]{0:T(1024)(128)(4,1)} %bitcast.387), calls=%async_computation.12 | async-start | bytes 8388608
  297.9 11.8 %slice-start.4 = ((s8[12582912]{0:T(1024)(128)(4,1)}), s8[4194304]{0:T(1024)(128)(4,1)S(1)}, s32[]{:S(2)}) async-start(s8[12582912]{0:T(1024)(128)(4,1)} %bitcast.387), calls=%async_computation.13 | async-start | bytes 8388608
  317.0 6.4 %copy-start = (bf16[2,512,3072]{2,1,0:T(8,128)(2,1)}, bf16[2,512,3072]{2,1,0:T(8,128)(2,1)S(1)}, u32[]{:S(2)}) copy-start(bf16[2,512,3072]{2,1,0:T(8,128)(2,1)S(1)} %multiply_convert_fusion) | copy-start | bytes 18874372
  371.7 5.1 copy-start.69
  389.6 5.0 copy-start.47
  389.6 5.0 copy-start.52
  389.6 5.0 copy-start.60
  389.6 5.0 copy-start.61
  389.6 5.1 copy-start.48
  389.6 5.1 copy-start.58
  389.6 5.1 copy-start.59
  389.7 5.1 copy-start.49
  389.7 5.1 copy-start.56
  389.7 5.1 copy-start.57
  389.7 5.1 copy-start.50
  389.7 5.1 copy-start.54
  389.7 5.1 copy-start.55
  389.7 5.1 copy-start.42
  389.7 5.2 copy-start.43
  389.7 5.2 copy-start.45
  389.7 5.2 copy-start.46
  414.2 51.1 %all-to-all-start.2 = ((bf16[16,192,2,224]{3,1,2,0:T(8,128)(2,1)}), bf16[16,192,2,224]{3,1,2,0:T(8,128)(2,1)}, u32[]{:S(2)}, u32[]{:S(2)}) async-start(bf16[16,192,2,224]{3,1,2,0:T(8,128)(2,1)} %copy.91), calls=%async_computation.2 | async-start | bytes 6291456 | tf_op jit(solution)/shard_map/all_to_all | solution.py:176
  423.8 7.3 %copy-start.10 = (bf16[3072,2,16]{0,2,1:T(8,128)(2,1)S(1)}, bf16[3072,2,16]{0,2,1:T(8,128)(2,1)}, u32[]{:S(2)}) copy-start(bf16[3072,2,16]{0,2,1:T(8,128)(2,1)} %copy-done.8) | copy-start | bytes 589828
  423.8 7.3 %copy-start.13 = (bf16[3072,2,16]{0,2,1:T(8,128)(2,1)S(1)}, bf16[3072,2,16]{0,2,1:T(8,128)(2,1)}, u32[]{:S(2)}) copy-start(bf16[3072,2,16]{0,2,1:T(8,128)(2,1)} %copy-done.11) | copy-start | bytes 589828
  427.5 6.0 copy-start.5
  488.7 31.5 %all-to-all-start.4 = ((bf16[1,192,2,2048]{1,2,0,3:T(2,128)(2,1)}), bf16[1,192,2,2048]{1,2,0,3:T(2,128)(2,1)}, u32[]{:S(2)}, u32[]{:S(2)}) async-start(bf16[1,192,2,2048]{1,2,0,3:T(2,128)(2,1)} %copy.99), calls=%async_computation.4 | async-start | bytes 4194304 | tf_op jit(solution)/shard_map/all_to_all | solution.py:185
  493.1 126.7 %all-reduce.5.cloned.1.call-start = ((), (), s32[]{:S(2)}) async-start(), calls=%async_computation.6 | async-start | bytes 4194304 | tf_op jit(solution)/shard_map/psum | solution.py:187
  493.1 10.6 %slice-start = ((s8[6291456]{0:T(1024)(128)(4,1)}), s8[4194304]{0:T(1024)(128)(4,1)S(1)}, s32[]{:S(2)}) async-start(s8[6291456]{0:T(1024)(128)(4,1)} %bitcast.385), calls=%async_computation.9 | async-start | bytes 8388608
  495.5 8.2 %slice-start.1 = ((s8[6291456]{0:T(1024)(128)(4,1)}), s8[2097152]{0:T(1024)(128)(4,1)S(1)}, s32[]{:S(2)}) async-start(s8[6291456]{0:T(1024)(128)(4,1)} %bitcast.385), calls=%async_computation.10 | async-start | bytes 4194304
  503.7 20.2 %copy-start.36 = (bf16[8,1,96,1024]{3,0,2,1:T(8,128)(2,1)S(1)}, bf16[8,1,96,1024]{3,0,2,1:T(8,128)(2,1)}, u32[]{:S(2)}) copy-start(bf16[8,1,96,1024]{3,0,2,1:T(8,128)(2,1)} %reshape.977) | copy-start | bytes 4718596
  (43 other events, 124.8 us)
Sparse Core Ops, SparseCore 0:
  10.3 52.0 all-gather.7
  64.0 12.7 all-gather.11
  78.6 27.7 all-gather.9
  528.6 91.0 all-reduce.4
